TPU v7x, 128 devices: a whole 4x4x4 slice. The times are simulated.
128 devices in a mesh: rep: 2 (over z_hi), fs: 32 (over z_lo, y, x), tp: 2 (over core).
Axes of the slice: x: 4, y: 4, z: 4 (z_hi: 2, z_lo: 2; z = z_hi * 2 + z_lo), core: 2. Of those that a mesh axis runs over, the one named last changes fastest.
Arguments:
- resid: bfloat16 [65536, 2048], P(('rep', 'fs'), 'tp'), may hold values from -6 to 6
- gain_mix_in: float32 [2048], replicated, may hold values from 0.1 to 1.9
- u_weight: float32 [2048, 1024], P('fs', 'tp'), may hold values from -0.125 to 0.125
- v_weight: float32 [2048, 1024], P('fs', 'tp'), may hold values from -0.125 to 0.125
- u_scale: float32 [1024], P('tp'), may hold values from 0.5 to 2
- v_scale: float32 [1024], P('tp'), may hold values from 0.3 to 3
- v_gain: float32 [1024], P('tp'), may hold values from 0.1 to 1.9
- mix_matrix: float32 [16, 128, 128], P('tp'), may hold values from -0.5 to 0.5
- mix_bias: float32 [16, 128], P('tp'), may hold values from 0.1 to 1.9
- out_weight: float32 [1024, 2048], P('tp', 'fs'), may hold values from -0.1875 to 0.1875
- out_scale: float32 [2048], P('fs'), may hold values from 0.3 to 3
- gain_mix_out: float32 [2048], replicated, may hold values from 0.1 to 1.9
- gain_ffn_in: float32 [2048], replicated, may hold values from 0.1 to 1.9
- up_weight: float32 [2048, 4096], P('fs', 'tp'), may hold values from -0.125 to 0.125
- up_scale: float32 [4096], P('tp'), may hold values from 0.5 to 2
- down_weight: float32 [4096, 2048], P('tp', 'fs'), may hold values from -0.09375 to 0.09375
- down_scale: float32 [2048], P('fs'), may hold values from 0.3 to 3
- gain_ffn_out: float32 [2048], replicated, may hold values from 0.1 to 1.9
Outputs:
- result: bfloat16 [65536, 2048], P(('rep', 'fs'), 'tp')
All inputs are finite; a program needn't handle non-finite values.
Results may differ from a plain program's by a relative error of at most 0.013.
Values may be sent and summed in bfloat16 or wider, within the bound.
No kernel may reach another device: no remote copies, remote signals or barrier semaphores. Data moves between devices by JAX's collectives and lax.ppermute only.
A program may use at most 128 MiB of HBM per device.

v0:
```python
import jax
import jax.numpy as jnp
from jax import lax
from jax.sharding import PartitionSpec as P


def turned_gather(arrays, axis, dims):
    turned = [jnp.moveaxis(a, dim, 0) for a, dim in zip(arrays, dims)]
    widths = [t[0].size for t in turned]
    both = jnp.concatenate([t.reshape(-1, w) for t, w in zip(turned, widths)], axis=1)
    result = lax.all_gather(both, axis, axis=0, tiled=True)
    pieces = jnp.split(result, [sum(widths[:k]) for k in range(1, len(widths))], axis=1)
    return tuple(
        (
            jnp.moveaxis(b.reshape(-1, *t.shape[1:]), 0, dim)
            for b, t, dim in zip(pieces, turned, dims)
        )
    )


def in_one_piece(arrays, axis, dim, along):
    ends, at = ([], 0)
    for a in arrays[:-1]:
        at += a.shape[along]
        ends.append(at)
    both = jnp.concatenate(arrays, axis=along)
    return tuple(jnp.split(lax.all_gather(both, axis, axis=dim, tiled=True), ends, axis=along))


def copy_for_each(array, axis):
    copies = jnp.broadcast_to(array, (lax.axis_size(axis), *array.shape))
    return lax.all_to_all(copies, axis, split_axis=0, concat_axis=0, tiled=True)


def over_copies(array, axis):
    return copy_for_each(array, axis).sum(axis=0)


def packed_total(arrays, axis):
    vector, at, gathered = (jnp.concatenate([a.reshape(-1) for a in arrays]), 0, [])
    running = over_copies(vector, axis)
    for a in arrays:
        gathered.append(running[at : at + a.size].reshape(a.shape))
        at += a.size
    return tuple(gathered)


def in_order(pieces, dim):
    dims = list(pieces.shape[1:])
    dims[dim] *= pieces.shape[0]
    return jnp.moveaxis(pieces, 0, dim).reshape(dims)


def gathered_copies(array, axis, dim):
    pieces = copy_for_each(array, axis)
    return in_order(pieces, dim)


def total_of_pieces(array, axis):
    pieces = lax.all_gather(array, axis).astype(jnp.float32)
    return pieces.sum(axis=0)


def in_blocks(array, dim, peers):
    before, after = (array.shape[:dim], array.shape[dim + 1 :])
    return jnp.moveaxis(array.reshape(*before, peers, -1, *after), dim, 0)


def sent_and_summed(array, axis, dim):
    peers = lax.axis_size(axis)
    pieces = lax.all_to_all(in_blocks(array, dim, peers), axis, 0, 0, tiled=True)
    return jnp.sum(pieces.astype(jnp.float32), axis=0)


def rms_norm(values, gain, width, power_sum):
    return values * lax.rsqrt(power_sum / width + 1e-06) * gain


def local(
    resid,
    gain_mix_in,
    u_weight,
    v_weight,
    u_scale,
    v_scale,
    v_gain,
    mix_matrix,
    mix_bias,
    out_weight,
    out_scale,
    gain_mix_out,
    gain_ffn_in,
    up_weight,
    up_scale,
    down_weight,
    down_scale,
    gain_ffn_out,
):
    rows = resid.shape[0]
    part_width = resid.shape[1]
    width = part_width * lax.axis_size("tp")
    lane = lax.axis_index("tp")
    full_rows = lax.all_gather(resid, "tp", axis=1, tiled=True)
    out_scales, down_scales = turned_gather((out_scale, down_scale), "fs", (0, 0))
    full_float = full_rows.astype(jnp.float32)
    normed = rms_norm(
        full_float, gain_mix_in, width, jnp.sum(full_float * full_float, axis=1, keepdims=True)
    ).astype(jnp.bfloat16)
    branch_cols = u_weight.shape[1]
    pieces = in_one_piece(
        (u_weight.astype(jnp.bfloat16), v_weight.astype(jnp.bfloat16)), "fs", 0, 1
    )
    u_pre = jnp.dot(normed, pieces[0], preferred_element_type=jnp.float32)
    v_pre = jnp.dot(normed, pieces[1], preferred_element_type=jnp.float32)
    u_act = jax.nn.gelu(u_pre * u_scale)
    v_act = jax.nn.gelu(v_pre * v_scale)
    total, squares = packed_total(
        (jnp.sum(v_act, axis=1, keepdims=True), jnp.sum(v_act * v_act, axis=1, keepdims=True)), "tp"
    )
    branch_width = branch_cols * lax.axis_size("tp")
    centre = total / branch_width
    spread = squares / branch_width - centre * centre
    v_norm = ((v_act - centre) * lax.rsqrt(spread + 1e-06) * v_gain).astype(jnp.bfloat16)
    groups = mix_matrix.shape[0]
    block = mix_matrix.shape[1]
    blocks = v_norm.reshape(rows // block, block, groups, branch_cols // groups)
    mixed = (
        jnp.einsum(
            "gts,bsgd->btgd",
            mix_matrix.astype(jnp.bfloat16),
            blocks,
            preferred_element_type=jnp.float32,
        )
        + mix_bias.T[None, :, :, None]
    )
    gated = (u_act * mixed.reshape(rows, branch_cols)).astype(jnp.bfloat16)
    partial_value = jnp.dot(
        gated,
        gathered_copies(out_weight.astype(jnp.bfloat16), "fs", 1),
        preferred_element_type=jnp.float32,
    )
    mix_out = (
        total_of_pieces(partial_value.astype(jnp.bfloat16), "tp").astype(jnp.float32) * out_scales
    )
    power = jnp.sum(mix_out * mix_out, axis=1, keepdims=True)
    middle_full = (full_float + rms_norm(mix_out, gain_mix_out, width, power)).astype(jnp.bfloat16)
    middle = lax.dynamic_slice_in_dim(middle_full, lane * part_width, part_width, 1)
    middle_float = middle_full.astype(jnp.float32)
    ffn_in = rms_norm(
        middle_float,
        gain_ffn_in,
        width,
        jnp.sum(middle_float * middle_float, axis=1, keepdims=True),
    ).astype(jnp.bfloat16)
    up_half = up_weight.astype(jnp.bfloat16)
    down_half = down_weight.astype(jnp.bfloat16)
    whole_up = lax.all_gather(up_half, "fs", axis=0, tiled=True)
    raised = jnp.dot(ffn_in, whole_up, preferred_element_type=jnp.float32)
    hidden = jnp.square(jax.nn.relu(raised * up_scale)).astype(jnp.bfloat16)
    whole_down = lax.all_gather(down_half, "fs", axis=1, tiled=True)
    terms = jnp.dot(hidden, whole_down, preferred_element_type=jnp.float32)
    own_down = lax.dynamic_slice_in_dim(down_scales, lane * part_width, part_width, 0)
    ffn_out = sent_and_summed(terms.astype(jnp.bfloat16), "tp", 1) * own_down
    power_out = over_copies(jnp.sum(ffn_out * ffn_out, axis=1, keepdims=True), "tp")
    own_gain_out = lax.dynamic_slice_in_dim(gain_ffn_out, lane * part_width, part_width, 0)
    return (middle.astype(jnp.float32) + rms_norm(ffn_out, own_gain_out, width, power_out)).astype(
        jnp.bfloat16
    )


def solution(mesh):
    in_specs = (
        P(("rep", "fs"), "tp"),
        P(),
        P("fs", "tp"),
        P("fs", "tp"),
        P("tp"),
        P("tp"),
        P("tp"),
        P("tp", None, None),
        P("tp", None),
        P("tp", "fs"),
        P("fs"),
        P(),
        P(),
        P("fs", "tp"),
        P("tp"),
        P("tp", "fs"),
        P("fs"),
        P(),
    )
    out_specs = P(("rep", "fs"), "tp")
    return jax.shard_map(local, mesh=mesh, in_specs=in_specs, out_specs=out_specs, check_vma=False)
```

profile of v0, /device:TPU:1, one launch (start us, length us, event | category | flops | bytes accessed | tf_op | source)
XLA Modules:
  0.0 657.6 jit_solution(17726470480720936505)
XLA Ops:
  6.5 0.7 all-gather.8.cloned.1.call-update
  7.3 0.0 all-gather.10.cloned.1.call-start
  7.3 0.9 convert_element_type.62
  8.2 0.9 convert_element_type.63
  9.1 0.7 pad_maximum_fusion
  9.8 0.0 all-gather.10.cloned.1.call-update
  9.8 0.9 convert_element_type.67
  10.8 18.3 %all-gather.8.cloned.1.call-done = bf16[1024,2048]{1,0:T(8,128)(2,1)} async-done(((bf16[1024,1024]{1,0:T(8,128)(2,1)}), bf16[1024,2048]{1,0:T(8,128)(2,1)}) %all-gather.8.cloned.1.call-update) | async-done | bytes 4194320 | tf_op jit(solution)/shard_map/all_gather | solution.py:103
  29.0 3.1 fusion.3
  32.1 135.9 %all-gather.10.cloned.1.call-done = bf16[2048,1024]{1,0:T(8,128)(2,1)} async-done(((bf16[64,1024]{1,0:T(8,128)(2,1)}), bf16[2048,1024]{1,0:T(8,128)(2,1)}) %all-gather.10.cloned.1.call-update) | async-done | bytes 4194320 | tf_op jit(solution)/shard_map/all_gather | solution.py:27
  168.0 5.8 fusion.68
  173.8 24.0 %all_to_all.21 = f32[2,1,2048]{2,1,0:T(1,128)S(1)} all-to-all(f32[2,1,2048]{2,1,0:T(1,128)S(1)} %broadcast_in_dim.6), channel_id=1, replica_groups=mesh['rep'=2,'fs'=32,'tp'=2] {'tp'}, dimensions={0} | all-to-all | bytes 32768 | tf_op jit(solution)/shard_map/all_to_all | solution.py:32
  197.8 1.6 broadcast_in_dim.7
  199.4 7.1 %all-to-all-start.1 = ((bf16[32,512,64]{1,2,0:T(8,128)(2,1)}), bf16[32,512,64]{1,2,0:T(8,128)(2,1)}, u32[]{:S(2)}, u32[]{:S(2)}) async-start(bf16[32,512,64]{1,2,0:T(8,128)(2,1)} %broadcast_in_dim.7), calls=%async_computation.1 | async-start | bytes 4194304 | tf_op jit(solution)/shard_map/all_to_all | solution.py:32
  206.5 0.0 all-gather.16.cloned.1.call-start
  206.6 0.3 multiply_convert_fusion.1
  206.9 2.1 reshape.90
  209.1 2.4 bitcast_add_fusion
  211.5 2.7 copy.55
  214.2 3.4 reshape.91
  217.6 15.7 %all-to-all-done.1 = bf16[32,512,64]{1,2,0:T(8,128)(2,1)} async-done(((bf16[32,512,64]{1,2,0:T(8,128)(2,1)}), bf16[32,512,64]{1,2,0:T(8,128)(2,1)}, u32[]{:S(2)}, u32[]{:S(2)}) %all-to-all-start.1) | async-done | bytes 2097184 | tf_op jit(solution)/shard_map/all_to_all | solution.py:32
  233.4 10.3 %convolution_convert_fusion = bf16[1024,2048]{1,0:T(8,128)(2,1)} fusion(bf16[512,2048]{0,1:T(8,128)(2,1)} %bitcast.5, f32[1024,512]{1,0:T(8,128)S(1)} %reshape.91, bf16[2048,1024]{1,0:T(8,128)(2,1)} %all-gather.10.cloned.1.call-done, bf16[1024,2048]{1,0:T(8,128)(2,1)} %all-gather.8.cloned.1.call-done, f32[2048]{0:T(1024)S(1)} %copy-done.10, ...), kind=kOutput, calls=%fused_computation.24 | convolution fusion | flops 4311220224 | bytes 14694400 | tf_op jit(solution)/shard_map/dot_general | solution.py:137
  243.7 0.0 all-gather.16.cloned.1.call-update
  243.8 0.0 all-gather.12.cloned.1.call-start
  243.8 1.0 copy-done.3
  244.8 0.7 convert_element_type.74
  245.5 0.0 all-gather.12.cloned.1.call-update
  245.5 0.0 all-gather.14.cloned.1.call-start
  245.6 0.7 convert_element_type.76
  246.3 0.0 all-gather.14.cloned.1.call-update
  246.4 66.4 %all-gather.1 = f32[32,64,2]{1,2,0:T(2,128)S(1)} all-gather(f32[1,64,2]{1,2,0:T(2,128)S(1)} %maximum_bitcast_fusion), channel_id=1, replica_groups=mesh['rep'=2,'fs'=32,'tp'=2] {'fs'}, dimensions={0}, use_global_device_ids=true | all-gather | bytes 16896 | tf_op jit(solution)/shard_map/all_gather | solution.py:11
  312.8 0.1 reshape.88
  312.9 0.0 all-gather.16.cloned.1.call-done
  313.0 9.9 %convert_reduce_fusion = f32[1024,2048]{1,0:T(8,128)} fusion(bf16[2,1024,2048]{2,1,0:T(8,128)(2,1)} %bitcast.34), kind=kLoop, calls=%fused_computation | loop fusion | flops 6291456 | bytes 16777216 | tf_op jit(solution)/shard_map/reduce_sum | solution.py:61
  322.9 4.5 multiply_reduce_fusion
  327.5 1.3 copy-done
  328.8 4.0 fusion
  332.8 82.2 %all-gather.12.cloned.1.call-done = bf16[2048,2048]{1,0:T(8,128)(2,1)} async-done(((bf16[64,2048]{1,0:T(8,128)(2,1)}), bf16[2048,2048]{1,0:T(8,128)(2,1)}) %all-gather.12.cloned.1.call-update) | async-done | bytes 8388624 | tf_op jit(solution)/shard_map/all_gather | solution.py:157
  415.0 167.9 %all-gather.14.cloned.1.call-done = bf16[2048,2048]{0,1:T(8,128)(2,1)} async-done(((bf16[2048,64]{0,1:T(8,128)(2,1)}), bf16[2048,2048]{0,1:T(8,128)(2,1)}) %all-gather.14.cloned.1.call-update) | async-done | bytes 8388624 | tf_op jit(solution)/shard_map/all_gather | solution.py:160
  582.9 25.7 %fusion.16 = bf16[1024,2048]{1,0:T(8,128)(2,1)} fusion(bf16[2048,2048]{0,1:T(8,128)(2,1)} %all-gather.14.cloned.1.call-done, bf16[2048,2048]{1,0:T(8,128)(2,1)} %all-gather.12.cloned.1.call-done, bf16[1024,2048]{1,0:T(8,128)(2,1)} %get-tuple-element.8, f32[2048]{0:T(1024)S(1)} %copy-done.11, f32[2048]{0:T(1024)S(1)} %copy-done.12, f32[1024]{0:T(1024)S(1)} %add_rsqrt_fusion.1), kind=kOutput, calls=%fused_computation.25 | convolution fusion | flops 17198743552 | bytes 25186304 | tf_op jit(solution)/shard_map/dot_general | solution.py:161
  608.5 2.6 copy.66
  611.2 27.7 %all_to_all.22 = bf16[2,1024,1024]{2,1,0:T(8,128)(2,1)S(1)} all-to-all(bf16[2,1024,1024]{2,1,0:T(8,128)(2,1)S(1)} %bitcast.33), channel_id=1, replica_groups=mesh['rep'=2,'fs'=32,'tp'=2] {'tp'}, dimensions={0} | all-to-all | bytes 8388608 | tf_op jit(solution)/shard_map/all_to_all | solution.py:71
  638.8 1.0 convert_reduce_fusion.1
  639.9 0.0 dynamic-slice-start
  639.9 1.9 copy-done.1
  641.8 0.5 multiply_reduce_fusion.1
  642.3 3.7 all_to_all.23
  646.1 5.0 add_convert_fusion
  (43 shorter events, 0.2 us)
Async XLA Ops:
  6.5 161.5 %copy-start.10 = (f32[2048]{0:T(1024)S(1)}, f32[2048]{0:T(1024)}, u32[]{:S(2)}) copy-start(f32[2048]{0:T(1024)} %param.19) | copy-start | bytes 24580
  6.5 161.5 %copy-start.13 = (f32[512]{0:T(512)S(1)}, f32[512]{0:T(512)}, u32[]{:S(2)}) copy-start(f32[512]{0:T(512)} %param.23) | copy-start | bytes 6148
  6.5 22.5 %all-gather.8.cloned.1.call-start = ((), (), s32[]{:S(2)}) async-start(), calls=%async_computation.4 | async-start | bytes 6291456 | tf_op jit(solution)/shard_map/all_gather | solution.py:103
  7.3 160.7 %all-gather.10.cloned.1.call-start = ((), (), s32[]{:S(2)}) async-start(), calls=%async_computation.5 | async-start | bytes 4325376 | tf_op jit(solution)/shard_map/all_gather | solution.py:27
  173.8 32.8 %copy-start.7 = (f32[512]{0:T(512)S(1)}, f32[512]{0:T(512)}, u32[]{:S(2)}) copy-start(f32[512]{0:T(512)} %param.24) | copy-start | bytes 6148
  199.4 34.0 %all-to-all-start.1 = ((bf16[32,512,64]{1,2,0:T(8,128)(2,1)}), bf16[32,512,64]{1,2,0:T(8,128)(2,1)}, u32[]{:S(2)}, u32[]{:S(2)}) async-start(bf16[32,512,64]{1,2,0:T(8,128)(2,1)} %broadcast_in_dim.7), calls=%async_computation.1 | async-start | bytes 4194304 | tf_op jit(solution)/shard_map/all_to_all | solution.py:32
  206.5 2.6 copy-start.6
  206.5 106.5 %all-gather.16.cloned.1.call-start = ((), (), s32[]{:S(2)}) async-start(), calls=%async_computation.8 | async-start | bytes 12582912 | tf_op jit(solution)/shard_map/all_gather | solution.py:60
  214.2 19.2 %copy-start.14 = (f32[512]{0:T(512)S(1)}, f32[512]{0:T(512)}, u32[]{:S(2)}) copy-start(f32[512]{0:T(512)} %param.22) | copy-start | bytes 6148
  243.7 1.0 copy-start.3
  243.7 1.9 copy-start.4
  243.7 2.6 copy-start.8
  243.7 2.6 copy-start.9
  243.8 171.2 %all-gather.12.cloned.1.call-start = ((), (), s32[]{:S(2)}) async-start(), calls=%async_computation.6 | async-start | bytes 8650752 | tf_op jit(solution)/shard_map/all_gather | solution.py:157
  245.5 337.3 %all-gather.14.cloned.1.call-start = ((), (), s32[]{:S(2)}) async-start(), calls=%async_computation.7 | async-start | bytes 8650752 | tf_op jit(solution)/shard_map/all_gather | solution.py:160
  313.0 14.5 %copy-start.2 = (bf16[1024,2048]{1,0:T(8,128)(2,1)S(1)}, bf16[1024,2048]{1,0:T(8,128)(2,1)}, u32[]{:S(2)}) copy-start(bf16[1024,2048]{1,0:T(8,128)(2,1)} %all-gather.8.cloned.1.call-done) | copy-start | bytes 12582916
  322.9 5.9 copy-start
  322.9 5.9 copy-start.5
  328.8 254.1 %copy-start.11 = (f32[2048]{0:T(1024)S(1)}, f32[2048]{0:T(1024)}, u32[]{:S(2)}) copy-start(f32[2048]{0:T(1024)} %param.32) | copy-start | bytes 24580
  328.8 254.1 %copy-start.12 = (f32[2048]{0:T(1024)S(1)}, f32[2048]{0:T(1024)}, u32[]{:S(2)}) copy-start(f32[2048]{0:T(1024)} %param.30) | copy-start | bytes 24580
  639.9 1.9 copy-start.1
  639.9 6.2 dynamic-slice-start
Sparse Core Ops, SparseCore 0:
  9.0 19.9 all-gather.7
  30.7 137.2 all-gather.9
  243.9 22.8 all-gather.15
  268.3 146.6 all-gather.11
  416.4 166.3 all-gather.13
where the time goes:
time: 658 us
  waiting for transfers between devices  421 us (64%)
  blocking collectives  122 us (19%)
  matrix products  44.2 us (7%)
  other arithmetic  33.3 us (5%)
  local copies, waits for them, and re-layouts  16.9 us (3%)
  between operations  13.4 us (2%)
  starting transfers between devices  7.24 us (1%)
    all_gather x1, waiting for transfers between devices, local(): whole_down = lax.all_gather(down_half, 'fs', axis=1, tiled=True)  168 us
    all_gather x1, waiting for transfers between devices, in_one_piece(): lax.all_gather(both, axis, axis=dim, tiled=True)  136 us
    all_gather x1, waiting for transfers between devices, local(): whole_up = lax.all_gather(up_half, 'fs', axis=0, tiled=True)  82.2 us
    all_gather x1, blocking collectives, turned_gather(): result = lax.all_gather(both, axis, axis=0, tiled=True)  66.4 us
    all_to_all x2, blocking collectives, copy_for_each(): return lax.all_to_all(copies, axis, split_axis=0, concat_axis=0, tiled=True)  27.7 us
    all_to_all x1, blocking collectives, sent_and_summed(): lax.all_to_all(in_blocks(array, dim, peers), axis, 0, 0, tiled=True)  27.7 us
    dot_general x1, matrix products, local(): terms = jnp.dot(hidden, whole_down, preferred_element_type=jnp.float32)  25.7 us
    all_gather x1, waiting for transfers between devices, local(): full_rows = lax.all_gather(resid, 'tp', axis=1, tiled=True)  18.3 us
  transfers between devices with their start and end apart: 6, of which 5 were waited for; matrix products, arithmetic and copies ran while one was open for 6% of the time, Pallas kernels for 0%

commit v1 on v0

--- a/solution.py
+++ b/solution.py
@@ -157,7 +157,8 @@
     whole_up = lax.all_gather(up_half, "fs", axis=0, tiled=True)
     raised = jnp.dot(ffn_in, whole_up, preferred_element_type=jnp.float32)
     hidden = jnp.square(jax.nn.relu(raised * up_scale)).astype(jnp.bfloat16)
-    whole_down = lax.all_gather(down_half, "fs", axis=1, tiled=True)
+    parts = lax.all_gather(down_half, "fs", axis=0, tiled=False)
+    whole_down = jnp.concatenate(parts, axis=1)
     terms = jnp.dot(hidden, whole_down, preferred_element_type=jnp.float32)
     own_down = lax.dynamic_slice_in_dim(down_scales, lane * part_width, part_width, 0)
     ffn_out = sent_and_summed(terms.astype(jnp.bfloat16), "tp", 1) * own_down

time: 658 us -> 628 us (0.954); the launches traced: 658 us -> 619 us
  waiting for transfers between devices: 421 us -> 354 us
  local copies, waits for them, and re-layouts: 16.9 us -> 40.2 us
    all_gather x1, waiting for transfers between devices: 168 us -> 24.6 us  [local(): parts = lax.all_gather(down_half, 'fs', axis=0, tiled=False)]
    all_gather x1, waiting for transfers between devices: 82.2 us -> 128 us  [local(): whole_up = lax.all_gather(up_half, 'fs', axis=0, tiled=True)]
    all_gather x1, waiting for transfers between devices: 0.02 us -> 19 us  [total_of_pieces(): pieces = lax.all_gather(array, axis).astype(jnp.float32)]
    all_to_all x1, waiting for transfers between devices: 15.7 us -> 28.9 us  [copy_for_each(): return lax.all_to_all(copies, axis, split_axis=0, concat_axis=0, tiled=True)]
    unnamed x31 -> x30, local copies, waits for them, and re-layouts: 4.35 us -> 16.4 us
    reshape x0 -> x1, local copies, waits for them, and re-layouts: none -> 11.2 us  [local(): whole_down = jnp.concatenate(parts, axis=1)]
  transfers between devices with their start and end apart: 6 -> 6, of which waited for: 5 -> 6; matrix products, arithmetic and copies ran while one was open for 6% -> 13% of each run, Pallas kernels for 0% -> 0%
where the time goes in v1:
time: 628 us; the launch traced here: 619 us
  waiting for transfers between devices  354 us (56%)
  blocking collectives  126 us (20%)
  matrix products  44.2 us (7%)
  local copies, waits for them, and re-layouts  40.2 us (6%)
  other arithmetic  34.5 us (5%)
  between operations  13.6 us (2%)
  starting transfers between devices  7.24 us (1%)
    all_gather x1, waiting for transfers between devices, in_one_piece(): lax.all_gather(both, axis, axis=dim, tiled=True)  136 us
    all_gather x1, waiting for transfers between devices, local(): whole_up = lax.all_gather(up_half, 'fs', axis=0, tiled=True)  128 us
    all_gather x1, blocking collectives, turned_gather(): result = lax.all_gather(both, axis, axis=0, tiled=True)  70 us
    all_to_all x1, waiting for transfers between devices, copy_for_each(): return lax.all_to_all(copies, axis, split_axis=0, concat_axis=0, tiled=True)  28.9 us
    all_to_all x1, blocking collectives, sent_and_summed(): lax.all_to_all(in_blocks(array, dim, peers), axis, 0, 0, tiled=True)  27.9 us
    all_to_all x2, blocking collectives, copy_for_each(): return lax.all_to_all(copies, axis, split_axis=0, concat_axis=0, tiled=True)  27.7 us
    dot_general x1, matrix products, local(): terms = jnp.dot(hidden, whole_down, preferred_element_type=jnp.float32)  25.7 us
    all_gather x1, waiting for transfers between devices, local(): parts = lax.all_gather(down_half, 'fs', axis=0, tiled=False)  24.6 us
  transfers between devices with their start and end apart: 6, of which 6 were waited for; matrix products, arithmetic and copies ran while one was open for 13% of the time, Pallas kernels for 0%

profile of v1, /device:TPU:1, one launch (start us, length us, event | category | flops | bytes accessed | tf_op | source)
XLA Modules:
  0.0 619.3 jit_solution(17536414373263872581)
XLA Ops:
  6.5 0.7 all-gather.9.cloned.1.call-update
  7.3 0.0 all-gather.11.cloned.1.call-start
  7.3 0.9 convert_element_type.62
  8.2 0.9 convert_element_type.63
  9.1 0.7 pad_maximum_fusion
  9.8 0.0 all-gather.11.cloned.1.call-update
  9.8 0.0 all-gather.17.cloned.1.call-start
  9.9 1.8 convert_element_type.76
  11.7 0.0 all-gather.17.cloned.1.call-update
  11.7 0.9 convert_element_type.67
  12.6 16.4 %all-gather.9.cloned.1.call-done = bf16[1024,2048]{1,0:T(8,128)(2,1)} async-done(((bf16[1024,1024]{1,0:T(8,128)(2,1)}), bf16[1024,2048]{1,0:T(8,128)(2,1)}) %all-gather.9.cloned.1.call-update) | async-done | bytes 4194320 | tf_op jit(solution)/shard_map/all_gather | solution.py:103
  29.0 3.1 fusion.3
  32.1 135.9 %all-gather.11.cloned.1.call-done = bf16[2048,1024]{1,0:T(8,128)(2,1)} async-done(((bf16[64,1024]{1,0:T(8,128)(2,1)}), bf16[2048,1024]{1,0:T(8,128)(2,1)}) %all-gather.11.cloned.1.call-update) | async-done | bytes 4194320 | tf_op jit(solution)/shard_map/all_gather | solution.py:27
  168.0 5.8 fusion.68
  173.8 24.0 %all_to_all.21 = f32[2,1,2048]{2,1,0:T(1,128)S(1)} all-to-all(f32[2,1,2048]{2,1,0:T(1,128)S(1)} %broadcast_in_dim.6), channel_id=1, replica_groups=mesh['rep'=2,'fs'=32,'tp'=2] {'tp'}, dimensions={0} | all-to-all | bytes 32768 | tf_op jit(solution)/shard_map/all_to_all | solution.py:32
  197.8 1.6 broadcast_in_dim.7
  199.4 7.1 %all-to-all-start.1 = ((bf16[32,512,64]{1,2,0:T(8,128)(2,1)}), bf16[32,512,64]{1,2,0:T(8,128)(2,1)}, u32[]{:S(2)}, u32[]{:S(2)}) async-start(bf16[32,512,64]{1,2,0:T(8,128)(2,1)} %broadcast_in_dim.7), calls=%async_computation.1 | async-start | bytes 4194304 | tf_op jit(solution)/shard_map/all_to_all | solution.py:32
  206.5 0.0 all-gather.15.cloned.1.call-start
  206.6 0.3 multiply_convert_fusion.1
  206.9 2.1 reshape.99
  209.1 2.4 bitcast_add_fusion
  211.5 2.8 copy.65
  214.2 3.4 reshape.100
  217.7 28.9 %all-to-all-done.1 = bf16[32,512,64]{1,2,0:T(8,128)(2,1)} async-done(((bf16[32,512,64]{1,2,0:T(8,128)(2,1)}), bf16[32,512,64]{1,2,0:T(8,128)(2,1)}, u32[]{:S(2)}, u32[]{:S(2)}) %all-to-all-start.1) | async-done | bytes 2097184 | tf_op jit(solution)/shard_map/all_to_all | solution.py:32
  246.5 10.4 %convolution_convert_fusion = bf16[1024,2048]{1,0:T(8,128)(2,1)} fusion(bf16[512,2048]{0,1:T(8,128)(2,1)} %bitcast.5, f32[1024,512]{1,0:T(8,128)S(1)} %reshape.100, bf16[2048,1024]{1,0:T(8,128)(2,1)} %all-gather.11.cloned.1.call-done, bf16[1024,2048]{1,0:T(8,128)(2,1)} %all-gather.9.cloned.1.call-done, f32[2048]{0:T(1024)S(1)} %copy-done.9, ...), kind=kOutput, calls=%fused_computation.24 | convolution fusion | flops 4311220224 | bytes 14694400 | tf_op jit(solution)/shard_map/dot_general | solution.py:137
  256.9 0.0 all-gather.15.cloned.1.call-update
  256.9 0.0 all-gather.13.cloned.1.call-start
  257.0 1.0 copy-done.3
  257.9 0.7 convert_element_type.74
  258.7 70.0 %all-gather.2 = f32[32,64,2]{1,2,0:T(2,128)S(1)} all-gather(f32[1,64,2]{1,2,0:T(2,128)S(1)} %maximum_bitcast_fusion), channel_id=1, replica_groups=mesh['rep'=2,'fs'=32,'tp'=2] {'fs'}, dimensions={0}, use_global_device_ids=true | all-gather | bytes 16896 | tf_op jit(solution)/shard_map/all_gather | solution.py:11
  328.8 0.1 reshape.97
  328.9 24.6 %all-gather.17.cloned.1.call-done = bf16[65536,64]{0,1:T(8,128)(2,1)} async-done(((bf16[2048,64]{0,1:T(8,128)(2,1)}), bf16[65536,64]{0,1:T(8,128)(2,1)}) %all-gather.17.cloned.1.call-update) | async-done | bytes 8388624 | tf_op jit(solution)/shard_map/all_gather | solution.py:160
  353.5 12.1 %copy.71 = bf16[8,8,32,2048]{3,2,1,0:T(8,128)(2,1)} copy(bf16[8,8,32,2048]{3,1,2,0:T(8,128)(2,1)} %bitcast.42) | data formatting | bytes 16777216
  365.6 11.2 %copy.59 = bf16[2048,32,64]{0,2,1:T(8,128)(2,1)} copy(bf16[2048,32,64]{0,1,2:T(8,128)(2,1)} %bitcast.40) | data formatting | bytes 16777216 | tf_op jit(solution)/shard_map/reshape | solution.py:161
  376.8 19.0 %all-gather.15.cloned.1.call-done = bf16[2048,2048]{1,0:T(8,128)(2,1)} async-done(((bf16[1024,2048]{1,0:T(8,128)(2,1)}), bf16[2048,2048]{1,0:T(8,128)(2,1)}) %all-gather.15.cloned.1.call-update) | async-done | bytes 8388624 | tf_op jit(solution)/shard_map/all_gather | solution.py:60
  395.8 10.0 %convert_reduce_fusion = f32[1024,2048]{1,0:T(8,128)} fusion(bf16[2,1024,2048]{2,1,0:T(8,128)(2,1)} %bitcast.43), kind=kLoop, calls=%fused_computation | loop fusion | flops 6291456 | bytes 16777216 | tf_op jit(solution)/shard_map/reduce_sum | solution.py:61
  405.8 4.5 multiply_reduce_fusion
  410.4 1.3 copy-done
  411.7 4.0 fusion
  415.7 128.4 %all-gather.13.cloned.1.call-done = bf16[2048,2048]{1,0:T(8,128)(2,1)} async-done(((bf16[64,2048]{1,0:T(8,128)(2,1)}), bf16[2048,2048]{1,0:T(8,128)(2,1)}) %all-gather.13.cloned.1.call-update) | async-done | bytes 8388624 | tf_op jit(solution)/shard_map/all_gather | solution.py:157
  544.1 25.7 %fusion.16 = bf16[1024,2048]{1,0:T(8,128)(2,1)} fusion(bf16[2048,2048]{0,1:T(8,128)(2,1)} %bitcast.44, bf16[2048,2048]{1,0:T(8,128)(2,1)} %all-gather.13.cloned.1.call-done, bf16[1024,2048]{1,0:T(8,128)(2,1)} %get-tuple-element.8, f32[2048]{0:T(1024)S(1)} %copy-done.10, f32[2048]{0:T(1024)S(1)} %copy-done.11, f32[1024]{0:T(1024)S(1)} %add_rsqrt_fusion.1), kind=kOutput, calls=%fused_computation.25 | convolution fusion | flops 17198743552 | bytes 25186304 | tf_op jit(solution)/shard_map/dot_general | solution.py:162
  569.8 2.6 copy.77
  572.4 27.9 %all_to_all.22 = bf16[2,1024,1024]{2,1,0:T(8,128)(2,1)S(1)} all-to-all(bf16[2,1024,1024]{2,1,0:T(8,128)(2,1)S(1)} %bitcast.41), channel_id=1, replica_groups=mesh['rep'=2,'fs'=32,'tp'=2] {'tp'}, dimensions={0} | all-to-all | bytes 8388608 | tf_op jit(solution)/shard_map/all_to_all | solution.py:71
  600.3 1.0 convert_reduce_fusion.1
  601.4 1.9 copy-done.1
  603.3 0.5 multiply_reduce_fusion.1
  603.8 3.7 all_to_all.23
  607.6 5.0 add_convert_fusion
  (43 shorter events, 0.2 us)
Async XLA Ops:
  6.5 161.5 %copy-start.9 = (f32[2048]{0:T(1024)S(1)}, f32[2048]{0:T(1024)}, u32[]{:S(2)}) copy-start(f32[2048]{0:T(1024)} %param.19) | copy-start | bytes 24580
  6.5 161.5 %copy-start.12 = (f32[512]{0:T(512)S(1)}, f32[512]{0:T(512)}, u32[]{:S(2)}) copy-start(f32[512]{0:T(512)} %param.23) | copy-start | bytes 6148
  6.5 22.5 %all-gather.9.cloned.1.call-start = ((), (), s32[]{:S(2)}) async-start(), calls=%async_computation.4 | async-start | bytes 6291456 | tf_op jit(solution)/shard_map/all_gather | solution.py:103
  7.3 160.7 %all-gather.11.cloned.1.call-start = ((), (), s32[]{:S(2)}) async-start(), calls=%async_computation.5 | async-start | bytes 4325376 | tf_op jit(solution)/shard_map/all_gather | solution.py:27
  9.8 343.7 %all-gather.17.cloned.1.call-start = ((), (), s32[]{:S(2)}) async-start(), calls=%async_computation.8 | async-start | bytes 8650752 | tf_op jit(solution)/shard_map/all_gather | solution.py:160
  173.8 32.8 %copy-start.6 = (f32[512]{0:T(512)S(1)}, f32[512]{0:T(512)}, u32[]{:S(2)}) copy-start(f32[512]{0:T(512)} %param.24) | copy-start | bytes 6148
  199.4 47.1 %all-to-all-start.1 = ((bf16[32,512,64]{1,2,0:T(8,128)(2,1)}), bf16[32,512,64]{1,2,0:T(8,128)(2,1)}, u32[]{:S(2)}, u32[]{:S(2)}) async-start(bf16[32,512,64]{1,2,0:T(8,128)(2,1)} %broadcast_in_dim.7), calls=%async_computation.1 | async-start | bytes 4194304 | tf_op jit(solution)/shard_map/all_to_all | solution.py:32
  206.5 2.6 copy-start.5
  206.5 189.3 %all-gather.15.cloned.1.call-start = ((), (), s32[]{:S(2)}) async-start(), calls=%async_computation.7 | async-start | bytes 12582912 | tf_op jit(solution)/shard_map/all_gather | solution.py:60
  214.2 32.3 %copy-start.13 = (f32[512]{0:T(512)S(1)}, f32[512]{0:T(512)}, u32[]{:S(2)}) copy-start(f32[512]{0:T(512)} %param.22) | copy-start | bytes 6148
  256.9 1.0 copy-start.3
  256.9 1.8 copy-start.7
  256.9 1.8 copy-start.8
  256.9 287.2 %all-gather.13.cloned.1.call-start = ((), (), s32[]{:S(2)}) async-start(), calls=%async_computation.6 | async-start | bytes 8650752 | tf_op jit(solution)/shard_map/all_gather | solution.py:157
  395.8 14.6 %copy-start.2 = (bf16[1024,2048]{1,0:T(8,128)(2,1)S(1)}, bf16[1024,2048]{1,0:T(8,128)(2,1)}, u32[]{:S(2)}) copy-start(bf16[1024,2048]{1,0:T(8,128)(2,1)} %all-gather.9.cloned.1.call-done) | copy-start | bytes 12582916
  405.8 5.9 copy-start
  405.8 5.9 copy-start.4
  411.7 132.4 %copy-start.10 = (f32[2048]{0:T(1024)S(1)}, f32[2048]{0:T(1024)}, u32[]{:S(2)}) copy-start(f32[2048]{0:T(1024)} %param.32) | copy-start | bytes 24580
  411.7 132.4 %copy-start.11 = (f32[2048]{0:T(1024)S(1)}, f32[2048]{0:T(1024)}, u32[]{:S(2)}) copy-start(f32[2048]{0:T(1024)} %param.30) | copy-start | bytes 24580
  601.3 1.9 copy-start.1
  601.4 6.2 %dynamic-slice-start = ((f32[2048]{0:T(1024)}, s32[]{:T(128)}), f32[1024]{0:T(1024)S(1)}, s32[]{:S(2)}) async-start(f32[2048]{0:T(1024)} %param.35, s32[]{:T(128)} %select_n.2), calls=%async_computation.9 | async-start | bytes 8704 | tf_op jit(solution)/shard_map/dynamic_slice | solution.py:166
Sparse Core Ops, SparseCore 0:
  9.0 19.9 all-gather.8
  30.7 137.2 all-gather.10
  169.6 183.7 all-gather.16
  355.0 40.7 all-gather.14
  397.3 146.7 all-gather.12
